TPU v7x, 32 devices: a whole 2x2x4 slice. The times are simulated.
32 devices in a mesh: sp: 4 (over z), fs: 4 (over y, x), tp: 2 (over core).
Axes of the slice: x: 2, y: 2, z: 4, core: 2. Of those that a mesh axis runs over, the one named last changes fastest.
Arguments:
- recurrent_query: bfloat16 [4, 1024, 1024], P('fs', 'sp', 'tp'), may hold values from -6 to 6
- forget_logits: bfloat16 [4, 1024, 1024], P('fs', 'sp', 'tp'), may hold values from -6 to 6
- recurrent_value: bfloat16 [4, 1024, 1024], P('fs', 'sp', 'tp'), may hold values from -6 to 6
- forget_floor: float32 [2, 1024], P(None, 'tp'), may hold values from 0.8 to 1
- extra_log_decay: float32 [4, 1024, 8], P('fs', 'sp', 'tp'), may hold values from -1 to 0
- recurrent_norm_gain: float32 [1024], P('tp'), may hold values from 0.1 to 1.9
- attention_query: bfloat16 [4, 1024, 768], P('fs', 'sp', 'tp'), may hold values from -300 to 300
- latent: bfloat16 [4, 1024, 256], P('fs', 'sp'), may hold values from -6 to 6
- rotary_key: bfloat16 [4, 1024, 32], P('fs', 'sp'), may hold values from -15 to 15
- latent_norm_gain: float32 [256], replicated, may hold values from 0.1 to 1.9
- latent_up_weight: bfloat16 [256, 1024], replicated, may hold values from -0.375 to 0.375
- recurrent_output_weight: bfloat16 [1024, 2048], P('tp', 'fs'), may hold values from -0.1875 to 0.1875
- attention_output_weight: bfloat16 [512, 2048], P('tp', 'fs'), may hold values from -2 to 2
Outputs:
- mixed: bfloat16 [4, 1024, 2048], P('fs', ('sp', 'tp'))
- log_weight: float32 [4, 1024, 8], P('fs', 'sp', 'tp')
All inputs are finite; a program needn't handle non-finite values.
Results may differ from a plain program's by a relative error of at most 0.013.
The roundings to bfloat16 on the way count: a program that leaves them out, or rounds other values in their place, can miss the bound.
Values may be sent and summed in bfloat16 or wider, within the bound.
A program may use at most 128 MiB of HBM per device.

v0:
```python
import math

import jax
import jax.numpy as jnp
from jax import lax
from jax.sharding import PartitionSpec as P

HG_DK = 128
HG_DV = 128
NOPE = 64
ROPE = 32
VDIM = 64
HG_BLOCK = 64
TOK_DEV = 256


norm_eps = 1e-06
rope_base = 10000.0
largest_value = lax.Precision.HIGHEST
widest_span = 8
floor_score = -1e30


def prefix(shard, axis, combine, identity, reverse):
    size, position = (lax.axis_size(axis), lax.axis_index(axis))
    everything = jax.tree.map(
        lambda part, kind: lax.all_gather(part.astype(kind), axis),
        shard,
        jax.tree.map(lambda a: jnp.bfloat16 if a.dtype == jnp.float32 else a.dtype, shard),
    )
    start = jax.tree.map(
        lambda part, zero: jnp.broadcast_to(jnp.asarray(zero, part.dtype), part.shape),
        shard,
        identity,
    )

    def hop(k, before):
        at = size - 1 - k if reverse else k
        reached = at > position if reverse else at < position
        new = combine(
            before, jax.tree.map(lambda part, own: part[at].astype(own.dtype), everything, shard)
        )
        return jax.tree.map(lambda a, b: jnp.where(reached, a, b), new, before)

    return lax.fori_loop(0, size, hop, start)


def from_partner(value, axis, distance):
    mask = 2**distance
    pairs = [(source, source ^ mask) for source in range(lax.axis_size(axis))]
    return lax.ppermute(value, axis, pairs)


def rope_tables(token_count, offset):
    places = offset + jnp.arange(token_count).astype(jnp.float32)
    pair_count = ROPE // 2
    inverse = rope_base ** (-jnp.arange(pair_count).astype(jnp.float32) / pair_count)
    angles = places[:, None] * inverse[None, :]
    return (jnp.cos(angles), jnp.sin(angles))


def rotate(tensor, cos_table, sin_table):
    half_width = tensor.shape[-1] // 2
    first_half = tensor[..., :half_width]
    second_half = tensor[..., half_width:]
    return jnp.concatenate(
        [
            first_half * cos_table - second_half * sin_table,
            first_half * sin_table + second_half * cos_table,
        ],
        axis=-1,
    )


def block_pass(queries, key_matrix, values, decay_logarithm, carried):
    length = queries.shape[0]
    blocks = length // HG_BLOCK

    def split_blocks(tensor):
        return tensor.reshape((blocks, HG_BLOCK) + tensor.shape[1:])

    lower_mask = jnp.tril(jnp.ones((HG_BLOCK, HG_BLOCK), dtype=bool))

    def advance(running_state, input_tuple):
        query_blk, key_tile, value_tile, decay_blk = input_tuple
        inner_block_term = jnp.cumsum(decay_blk, axis=0)
        damped_query = query_blk * jnp.exp(inner_block_term)
        key_decayed = key_tile * jnp.exp(-inner_block_term)
        cross_block_term = jnp.einsum(
            "mcx,cxn->mcn", damped_query, running_state, precision=largest_value
        )
        scores = jnp.einsum("thk,shk->hts", damped_query, key_decayed, precision=largest_value)
        scores = jnp.where(lower_mask[None], scores, 0.0)
        intra_term = jnp.einsum("hts,shv->thv", scores, value_tile, precision=largest_value)
        decay_total = inner_block_term[-1]
        updated_state = jnp.exp(decay_total)[:, :, None] * running_state + jnp.einsum(
            "jrg,jrb->rgb",
            key_tile * jnp.exp(decay_total[None] - inner_block_term),
            value_tile,
            precision=largest_value,
        )
        return (updated_state, cross_block_term + intra_term)

    final_state, outputs = lax.scan(
        advance,
        carried,
        (
            split_blocks(queries),
            split_blocks(key_matrix),
            split_blocks(values),
            split_blocks(decay_logarithm),
        ),
    )
    return (outputs.reshape((length,) + outputs.shape[2:]), final_state)


def gate_factors(forget_gate, spike_amount, gate_floor):
    decay_logarithm = (
        jnp.logaddexp(jnp.log(gate_floor), jnp.log1p(-gate_floor) + jax.nn.log_sigmoid(forget_gate))
        + spike_amount[:, :, None]
    )
    key_matrix = (1.0 - gate_floor) * jax.nn.sigmoid(-forget_gate)
    return (key_matrix, decay_logarithm)


def head_norm(outputs, gain):
    return (
        outputs * lax.rsqrt(jnp.mean(outputs * outputs, axis=-1, keepdims=True) + norm_eps) * gain
    )


def chain_combine(earlier, later):
    return (earlier[0] * later[0], later[0][:, :, None] * earlier[1] + later[1])


def local(
    recurrent_query,
    forget_logits,
    recurrent_value,
    forget_floor,
    extra_log_decay,
    recurrent_norm_gain,
    attention_query,
    latent,
    rotary_key,
    latent_norm_gain,
    latent_up_weight,
    recurrent_output_weight,
    attention_output_weight,
):
    span = min(lax.axis_size("sp"), widest_span)
    seq_len = TOK_DEV * span
    sp_index = lax.axis_index("sp")
    local_place = sp_index % span
    seq_offset = sp_index * TOK_DEV % seq_len
    queries = recurrent_query[0].astype(jnp.float32)
    heads_here = queries.shape[1] // HG_DK
    queries = queries.reshape(TOK_DEV, heads_here, HG_DK)
    forget_gate = forget_logits[0].astype(jnp.float32).reshape(TOK_DEV, heads_here, HG_DK)
    values = recurrent_value[0].astype(jnp.float32).reshape(TOK_DEV, heads_here, HG_DV)
    summed = jnp.zeros((TOK_DEV, heads_here, HG_DV), jnp.float32)
    for direction in range(2):
        gate_floor = forget_floor[direction].reshape(heads_here, HG_DK)
        key_matrix, decay_logarithm = gate_factors(forget_gate, extra_log_decay[0], gate_floor)
        sorted_rows = [queries, key_matrix, values, decay_logarithm]
        if direction == 1:
            sorted_rows = [jnp.flip(member, axis=0) for member in sorted_rows]
        local_out, local_state = block_pass(
            sorted_rows[0],
            sorted_rows[1],
            sorted_rows[2],
            sorted_rows[3],
            jnp.zeros((heads_here, HG_DK, HG_DV), jnp.float32),
        )
        running_state = jnp.cumsum(sorted_rows[3], axis=0)
        boundary = local_place == (span - 1 if direction == 0 else 0)
        element = (
            jnp.where(boundary, 0.0, jnp.exp(running_state[-1])),
            jnp.where(boundary, 0.0, local_state),
        )
        identity = (
            jnp.ones((heads_here, HG_DK), jnp.float32),
            jnp.zeros((heads_here, HG_DK, HG_DV), jnp.float32),
        )
        if direction == 0:
            arriving_state = prefix(element, "sp", chain_combine, identity, False)
        else:
            arriving_state = prefix(element, "sp", chain_combine, identity, True)
        result = local_out + jnp.einsum(
            "mcx,cxn->mcn",
            sorted_rows[0] * jnp.exp(running_state),
            arriving_state[1],
            precision=largest_value,
        )
        if direction == 1:
            result = jnp.flip(result, axis=0)
        summed = summed + result
    normed = head_norm(summed, recurrent_norm_gain.reshape(heads_here, HG_DV))
    recurrent_out = normed.astype(jnp.bfloat16).reshape(TOK_DEV, heads_here * HG_DV)
    heads_att = attention_query.shape[2] // (NOPE + ROPE)
    head_query = attention_query[0].reshape(TOK_DEV, heads_att, NOPE + ROPE)
    cos_table, sin_table = rope_tables(TOK_DEV, seq_offset.astype(jnp.float32))
    query_rope = rotate(
        head_query[..., NOPE:].astype(jnp.float32), cos_table[:, None], sin_table[:, None]
    )
    query_all = jnp.concatenate([head_query[..., :NOPE], query_rope.astype(jnp.bfloat16)], axis=-1)
    latent_wide = latent[0].astype(jnp.float32)
    normed = (
        latent_wide
        * lax.rsqrt(jnp.mean(latent_wide * latent_wide, axis=-1, keepdims=True) + norm_eps)
        * latent_norm_gain
    ).astype(jnp.bfloat16)
    rotated_key = rotate(rotary_key[0].astype(jnp.float32), cos_table, sin_table).astype(
        jnp.bfloat16
    )
    width_here = heads_att * (NOPE + VDIM)
    w_here = lax.dynamic_slice_in_dim(
        latent_up_weight, lax.axis_index("tp") * width_here, width_here, 1
    )
    score_scale = (NOPE + ROPE) ** (-0.5)

    def attend_keys(carried, expanded, rotated):
        key_count = expanded.shape[0]
        expanded = expanded.reshape(key_count, heads_att, NOPE + VDIM)
        keys_all = jnp.concatenate(
            [
                expanded[..., :NOPE],
                jnp.broadcast_to(rotated[:, None, :], (key_count, heads_att, ROPE)),
            ],
            axis=-1,
        )
        values = expanded[..., NOPE:]
        scores = jnp.einsum("qhd,khd->hqk", query_all, keys_all, preferred_element_type=jnp.float32)
        scores = scores * score_scale
        row_peak, totals, weighted = carried
        new_peak = jnp.maximum(row_peak, jnp.max(scores, axis=-1))
        weights = jnp.exp(scores - new_peak[..., None])
        rescale = jnp.exp(row_peak - new_peak)
        totals = totals * rescale + jnp.sum(weights, axis=-1)
        weighted = weighted * rescale.T[:, :, None] + jnp.einsum(
            "hqk,khv->qhv", weights.astype(jnp.bfloat16), values, preferred_element_type=jnp.float32
        )
        return (new_peak, totals, weighted)

    initial = (
        jnp.full((heads_att, TOK_DEV), floor_score, jnp.float32),
        jnp.zeros((heads_att, TOK_DEV), jnp.float32),
        jnp.zeros((TOK_DEV, heads_att, VDIM), jnp.float32),
    )
    pieces = (normed, rotated_key)
    for bit_number in range(span.bit_length() - 1):
        partner = from_partner((pieces[0], pieces[1]), "sp", bit_number)
        pieces = (
            jnp.concatenate([pieces[0], partner[0]], axis=0),
            jnp.concatenate([pieces[1], partner[1]], axis=0),
        )
    first_rows = pieces[0]
    rotated = pieces[1]
    key_count = first_rows.shape[0]
    key_block = math.gcd(key_count, max(TOK_DEV, 1024))
    grouped = (
        first_rows.reshape(key_count // key_block, key_block, first_rows.shape[1]),
        rotated.reshape(key_count // key_block, key_block, rotated.shape[1]),
    )

    def visit_block(running_state, block_parts):
        expanded = jnp.dot(block_parts[0], w_here, preferred_element_type=jnp.float32).astype(
            jnp.bfloat16
        )
        return (attend_keys(running_state, expanded, block_parts[1]), None)

    folded, unused = lax.scan(visit_block, initial, grouped)
    row_peak, totals, weighted = folded
    attention_attention_out = (
        (weighted / totals.T[:, :, None]).astype(jnp.bfloat16).reshape(TOK_DEV, heads_att * VDIM)
    )
    log_weight = (row_peak + jnp.log(totals)).T
    attention_out, log_weight = (attention_attention_out, log_weight)
    w_hg_full, w_att_full = (
        lax.all_gather(recurrent_output_weight, "fs", axis=1, tiled=True),
        lax.all_gather(attention_output_weight, "fs", axis=1, tiled=True),
    )
    rows_here = TOK_DEV // lax.axis_size("tp")
    mixed = lax.psum_scatter(
        (
            jnp.dot(recurrent_out, w_hg_full, preferred_element_type=jnp.float32)
            + jnp.dot(attention_out, w_att_full, preferred_element_type=jnp.float32)
        ).astype(jnp.bfloat16),
        "tp",
        scatter_dimension=0,
        tiled=True,
    )
    return (mixed.reshape(1, rows_here, mixed.shape[-1]), log_weight[None])


def solution(mesh):
    placed = (
        P("fs", "sp", "tp"),
        P("fs", "sp", "tp"),
        P("fs", "sp", "tp"),
        P(None, "tp"),
        P("fs", "sp", "tp"),
        P("tp"),
        P("fs", "sp", "tp"),
        P("fs", "sp", None),
        P("fs", "sp", None),
        P(),
        P(),
        P("tp", "fs"),
        P("tp", "fs"),
    )
    return jax.shard_map(
        local,
        mesh=mesh,
        in_specs=placed,
        out_specs=(P("fs", ("sp", "tp"), None), P("fs", "sp", "tp")),
        check_vma=False,
    )
```

profile of v0, /device:TPU:0, one launch (start us, length us, event | category | flops | bytes accessed | tf_op | source)
XLA Modules:
  0.0 191.9 jit_solution(15008523574658432252)
XLA Ops:
  10.1 3.1 %collective-permute-start.2 = (bf16[256,32]{0,1:T(8,128)(2,1)}, bf16[256,32]{0,1:T(8,128)(2,1)}, u32[]{:S(2)}, u32[]{:S(2)}) collective-permute-start(bf16[256,32]{0,1:T(8,128)(2,1)} %pad_maximum_fusion.3), channel_id=1, source_target_pairs={{0,8},{8,0},{16,24},{24,16},{1,9},{9,1},{17,25},{25,17},{2,10},{10... | collective-permute-start | bytes 49160 | tf_op jit(solution)/shard_map/ppermute | solution.py:51
  13.2 1.0 fusion.93
  14.2 1.0 fusion.95
  15.4 1.1 copy.150
  18.2 1.1 copy.148
  19.4 1.5 reshape.295
  25.1 1.5 copy.153
  26.6 2.0 %reshape.284 = f32[4,64,4,128]{3,2,1,0:T(4,128)} reshape(f32[1,256,512]{2,1,0:T(8,128)} %copy.151) | data formatting | bytes 1048576 | tf_op jit(solution)/shard_map/convert_element_type | solution.py:156
  28.7 3.5 %select_add_fusion.1 = (f32[4,64,4,128]{3,2,1,0:T(4,128)}, f32[4,64,4,128]{3,2,1,0:T(4,128)}) fusion(f32[4,64,4,128]{3,2,1,0:T(4,128)} %neg.73, f32[4,64,4]{2,1,0:T(8,128)S(1)} %bitcast.258, f32[4,128]{1,0:T(4,128)S(1)} %bitcast.262, f32[4,128]{1,0:T(4,128)S(1)} %bitcast.264, f32[4,64,4,128]{3,2,1,0:T(4,128)} %div.35, f32[4,128]{1,0:T(4,128)S(1)} %bitcast.272), kind=kLoop, calls=%fused_computation.121 | loop fusion | flops 2359296 | bytes 2107392 | tf_op jit(solution)/shard_map/add | solution.py:119
  33.0 17.6 %while.62 = (s32[]{:T(128)}, f32[4,128,128]{2,1,0:T(8,128)S(1)}, f32[4,64,4,128]{3,1,0,2:T(8,128)}, f32[4,64,4,128]{3,2,1,0:T(4,128)}, f32[4,64,4,128]{3,2,1,0:T...) while((s32[]{:T(128)}, f32[4,128,128]{2,1,0:T(8,128)S(1)}, ...), condition=%wide.region_2.3_spmd.clone, body=%wide.region_0.2_spmd.clone.sunk | while | flops 153538560 | bytes 3232884 | solution.py:104
  34.0 1.1 bitcast_multiply_fusion.7
  35.7 1.0 fusion.156
  38.4 1.1 bitcast_multiply_fusion.7
  40.1 1.0 fusion.156
  42.8 1.1 bitcast_multiply_fusion.7
  47.2 1.1 bitcast_multiply_fusion.7
  50.7 15.8 %all-gather = bf16[16,128,128]{2,1,0:T(8,128)(2,1)S(1)} all-gather(bf16[4,128,128]{2,1,0:T(8,128)(2,1)S(1)} %select_convert_fusion.1), channel_id=2, replica_groups=mesh['sp'=4,'fs'=4,'tp'=2] {'sp'}, dimensions={0}, use_global_device_ids=true | all-gather | bytes 655360 | tf_op jit(solution)/shard_map/all_gather | solution.py:27
  66.5 2.5 %add_bitcast_fusion = (f32[128,4,256]{2,0,1:T(8,128)}, f32[256,4,128]{0,2,1:T(8,128)S(1)}) fusion(f32[256,4]{0,1:T(4,128)} %bitcast.266, f32[4,128]{1,0:T(4,128)} %bitcast.263, f32[4,128]{1,0:T(4,128)} %bitcast.265, f32[256,4,128]{0,2,1:T(8,128)S(1)} %bitcast.234, f32[4,128]{1,0:T(4,128)} %bitcast.270, f32[4,128]{1,0:T(4,128)} %bitcast.271), kind=kLoop, calls=%fused_computation.120 | loop fusion | flops 3538944 | bytes 1585152 | tf_op jit(solution)/shard_map/transpose.4
  69.0 2.1 %copy.155 = f32[128,4,256]{0,2,1:T(8,128)} copy(f32[128,4,256]{2,0,1:T(8,128)} %get-tuple-element.581) | data formatting | bytes 1048576 | tf_op jit(solution)/shard_map/transpose.4
  71.1 1.4 fusion.87
  72.8 11.7 %all_gather.26 = bf16[4,4,128]{2,1,0:T(4,128)(2,1)S(1)} all-gather(bf16[1,4,128]{2,1,0:T(4,128)(2,1)S(1)} %copy.158), channel_id=1, replica_groups=mesh['sp'=4,'fs'=4,'tp'=2] {'sp'}, dimensions={0}, use_global_device_ids=true | all-gather | bytes 5120 | tf_op jit(solution)/shard_map/all_gather | solution.py:27
  87.4 1.4 fusion.85
  89.4 1.3 reduce-window.19
  92.4 7.6 %all_gather.29 = bf16[4,4,128]{2,1,0:T(4,128)(2,1)} all-gather(bf16[1,4,128]{2,1,0:T(4,128)(2,1)S(1)} %copy.174), channel_id=1, replica_groups=mesh['sp'=4,'fs'=4,'tp'=2] {'sp'}, dimensions={0}, use_global_device_ids=true | all-gather | bytes 5120 | tf_op jit(solution)/shard_map/all_gather | solution.py:27
  101.6 1.0 copy.163
  103.6 3.8 %rev.18 = f32[256,4,128]{0,2,1:T(8,128)S(1)} reverse(f32[256,4,128]{0,2,1:T(8,128)} %bitcast.248), dimensions={0} | reverse | bytes 1048576 | tf_op jit(solution)/shard_map/jit(_flip)/rev | solution.py:167
  108.5 14.3 %while.64 = (s32[]{:T(128)}, f32[4,128,128]{2,1,0:T(8,128)S(1)}, f32[4,64,4,128]{3,1,0,2:T(8,128)}, f32[4,64,4,128]{3,1,0,2:T(8,128)S(1)}, f32[4,64,4,128]{3,2,1...) while((s32[]{:T(128)}, f32[4,128,128]{2,1,0:T(8,128)S(1)}, ...), condition=%wide.region_9.10_spmd.clone, body=%wide.region_7.9_spmd.clone.sunk | while | flops 153538560 | bytes 3756664 | solution.py:104
  108.6 1.1 bitcast_multiply_fusion.8
  110.4 1.0 fusion.168
  112.2 1.1 bitcast_multiply_fusion.8
  113.9 1.0 fusion.168
  115.8 1.1 bitcast_multiply_fusion.8
  117.5 1.0 fusion.168
  119.3 1.1 bitcast_multiply_fusion.8
  121.1 1.0 fusion.168
  122.8 14.9 %all-gather.1 = bf16[16,128,128]{2,1,0:T(8,128)(2,1)S(1)} all-gather(bf16[4,128,128]{2,1,0:T(8,128)(2,1)S(1)} %select_convert_fusion), channel_id=3, replica_groups=mesh['sp'=4,'fs'=4,'tp'=2] {'sp'}, dimensions={0}, use_global_device_ids=true | all-gather | bytes 655360 | tf_op jit(solution)/shard_map/all_gather | solution.py:27
  137.6 3.6 %while.65 = (s32[]{:T(128)}, f32[4,128,128]{2,1,0:T(8,128)S(1)}, s32[]{:T(128)}, bf16[4,4,128]{2,1,0:T(4,128)(2,1)}, bf16[4,4,128,128]{3,2,1,0:T(8,128)(2,1)S(1)...) while((s32[]{:T(128)}, f32[4,128,128]{2,1,0:T(8,128)S(1)}, s32[]{:T(128)}, ...), condition=%wide.region_13.14_spmd.clone, body=%wide.region_12.13_spmd.clone.sunk | while | flops 328200 | bytes 660647 | solution.py:45
  141.3 2.1 %copy.176 = f32[256,4,128]{0,2,1:T(8,128)} copy(f32[256,4,128]{2,0,1:T(8,128)} %bitcast.249) | data formatting | bytes 1048576 | tf_op jit(solution)/shard_map/reshape | solution.py:114
  143.4 2.6 %fusion.57 = f32[256,4,128]{0,2,1:T(8,128)} fusion(f32[256,4,128]{0,2,1:T(8,128)} %copy.176, f32[4,128,128]{2,1,0:T(8,128)S(1)} %get-tuple-element.343, f32[256,4,128]{2,0,1:T(8,128)S(1)} %bitcast.233, f32[256,4,128]{2,0,1:T(8,128)} %bitcast.246), kind=kOutput, calls=%fused_computation.87 | convolution fusion | flops 201588736 | bytes 2359296 | tf_op jit(solution)/shard_map/mcx,cxn->mcn/dot_general | solution.py:189
  146.1 3.8 %rev.20 = f32[256,4,128]{0,2,1:T(8,128)S(1)} reverse(f32[256,4,128]{0,2,1:T(8,128)} %fusion.57), dimensions={0} | reverse | bytes 1048576 | tf_op jit(solution)/shard_map/jit(_flip)/rev | solution.py:196
  150.8 1.7 multiply_reduce_fusion.1
  152.6 1.1 copy.177
  156.9 2.3 %collective-permute-start.1 = (bf16[512,256]{1,0:T(8,128)(2,1)S(1)}, bf16[512,256]{1,0:T(8,128)(2,1)S(1)}, u32[]{:S(2)}, u32[]{:S(2)}) collective-permute-start(bf16[512,256]{1,0:T(8,128)(2,1)S(1)} %pad_maximum_fusion), channel_id=1, source_target_pairs={{0,16},{8,24},{16,0},{24,8},{1,17},{9,25},{17,1},{25,9},{2,18},{10... | collective-permute-start | bytes 786440 | tf_op jit(solution)/shard_map/ppermute | solution.py:51
  161.1 5.9 %collective-permute-done.1 = bf16[512,256]{1,0:T(8,128)(2,1)S(1)} collective-permute-done((bf16[512,256]{1,0:T(8,128)(2,1)S(1)}, bf16[512,256]{1,0:T(8,128)(2,1)S(1)}, u32[]{:S(2)}, u32[]{:S(2)}) %collective-permute-start.1) | collective-permute-done | bytes 262176 | tf_op jit(solution)/shard_map/ppermute | solution.py:51
  167.1 1.4 convolution_convert_fusion
  171.9 1.7 fusion.111
  173.6 3.3 %fusion.50 = bf16[256,2048]{1,0:T(8,128)(2,1)} fusion(f32[256,2048]{1,0:T(8,128)S(1)} %fusion.111, bf16[256,512]{0,1:T(8,128)(2,1)S(1)} %bitcast.255, bf16[512,2048]{1,0:T(8,128)(2,1)} %all-gather.5.cloned.1.call-done), kind=kOutput, calls=%fused_computation.76 | convolution fusion | flops 537919488 | bytes 5505024 | tf_op jit(solution)/shard_map/dot_general | solution.py:286
  177.0 8.4 %reduce-scatter.2.cloned.1.call-done = bf16[128,2048]{1,0:T(8,128)(2,1)} async-done(((bf16[256,2048]{1,0:T(8,128)(2,1)}), bf16[128,2048]{1,0:T(8,128)(2,1)}) %reduce-scatter.2.cloned.1.call-update) | async-done | bytes 524304 | tf_op jit(solution)/shard_map/reduce_scatter | solution.py:284
  (184 shorter events, 49.3 us)
Async XLA Ops:
  7.2 159.9 %copy-start = (bf16[256,1024]{1,0:T(8,128)(2,1)S(1)}, bf16[256,1024]{1,0:T(8,128)(2,1)}, u32[]{:S(2)}) copy-start(bf16[256,1024]{1,0:T(8,128)(2,1)} %param.31) | copy-start | bytes 1572868
  7.2 14.5 %copy-start.14 = (f32[2,512]{1,0:T(2,128)S(1)}, f32[2,512]{1,0:T(2,128)}, u32[]{:S(2)}) copy-start(f32[2,512]{1,0:T(2,128)} %param.24) | copy-start | bytes 12292
  7.2 15.1 %copy-start.10 = (bf16[1,256,512]{2,1,0:T(8,128)(2,1)S(1)}, bf16[1,256,512]{2,1,0:T(8,128)(2,1)}, u32[]{:S(2)}) copy-start(bf16[1,256,512]{2,1,0:T(8,128)(2,1)} %param.22) | copy-start | bytes 786436
  7.2 164.7 %all-gather.7.cloned.1.call-start = ((), (), s32[]{:S(2)}) async-start(), calls=%async_computation.2 | async-start | bytes 1310720 | tf_op jit(solution)/shard_map/all_gather | solution.py:281
  7.9 165.7 %all-gather.5.cloned.1.call-start = ((), (), s32[]{:S(2)}) async-start(), calls=%async_computation.1 | async-start | bytes 2621440 | tf_op jit(solution)/shard_map/all_gather | solution.py:280
  10.1 144.4 %collective-permute-start.2 = (bf16[256,32]{0,1:T(8,128)(2,1)}, bf16[256,32]{0,1:T(8,128)(2,1)}, u32[]{:S(2)}, u32[]{:S(2)}) collective-permute-start(bf16[256,32]{0,1:T(8,128)(2,1)} %pad_maximum_fusion.3), channel_id=1, source_target_pairs={{0,8},{8,0},{16,24},{24,16},{1,9},{9,1},{17,25},{25,17},{2,10},{10... | collective-permute-start | bytes 49160 | tf_op jit(solution)/shard_map/ppermute | solution.py:51
  15.2 140.8 %collective-permute-start = (bf16[256,256]{1,0:T(8,128)(2,1)S(1)}, bf16[256,256]{1,0:T(8,128)(2,1)}, u32[]{:S(2)}, u32[]{:S(2)}) collective-permute-start(bf16[256,256]{1,0:T(8,128)(2,1)S(1)} %fusion.95), channel_id=1, source_target_pairs={{0,8},{8,0},{16,24},{24,16},{1,9},{9,1},{17,25},{25,17},{2,10},{10... | collective-permute-start | bytes 393224 | tf_op jit(solution)/shard_map/ppermute | solution.py:51
  15.3 170.1 %reduce-scatter.2.cloned.1.call-start = ((), (), s32[]{:S(2)}) async-start(), calls=%async_computation.3 | async-start | bytes 1572864 | tf_op jit(solution)/shard_map/reduce_scatter | solution.py:284
  19.3 5.6 %copy-start.13 = (f32[1,256,4]{1,2,0:T(4,128)S(1)}, f32[1,256,4]{1,2,0:T(4,128)}, u32[]{:S(2)}) copy-start(f32[1,256,4]{1,2,0:T(4,128)} %param.25) | copy-start | bytes 12292
  22.3 6.4 %copy-start.11 = (f32[1,512]{1,0:T(1,128)}, f32[1,512]{1,0:T(1,128)S(1)}, u32[]{:S(2)}) copy-start(f32[1,512]{1,0:T(1,128)S(1)} %get-tuple-element.593) | copy-start | bytes 6148
  22.3 6.4 %copy-start.12 = (f32[1,512]{1,0:T(1,128)}, f32[1,512]{1,0:T(1,128)S(1)}, u32[]{:S(2)}) copy-start(f32[1,512]{1,0:T(1,128)S(1)} %get-tuple-element.597) | copy-start | bytes 6148
  22.6 9.6 %copy-start.1 = (f32[1,256,512]{1,2,0:T(8,128)}, f32[1,256,512]{1,2,0:T(8,128)S(1)}, u32[]{:S(2)}) copy-start(f32[1,256,512]{1,2,0:T(8,128)S(1)} %get-tuple-element.583) | copy-start | bytes 1572868
  72.8 11.7 %copy-start.5 = (f32[128,4,2,128]{0,3,2,1:T(8,128)}, f32[128,4,2,128]{0,3,2,1:T(8,128)S(1)}, u32[]{:S(2)}) copy-start(f32[128,4,2,128]{0,3,2,1:T(8,128)S(1)} %copy.157) | copy-start | bytes 1572868
  84.5 15.6 %copy-start.2 = (f32[1,256,512]{1,2,0:T(8,128)S(1)}, f32[1,256,512]{1,2,0:T(8,128)}, u32[]{:S(2)}) copy-start(f32[1,256,512]{1,2,0:T(8,128)} %copy-done.1) | copy-start | bytes 1572868
  86.2 16.5 %copy-start.8 = (f32[1,256,512]{1,2,0:T(8,128)S(1)}, f32[1,256,512]{1,2,0:T(8,128)}, u32[]{:S(2)}) copy-start(f32[1,256,512]{1,2,0:T(8,128)} %convert_element_type.188) | copy-start | bytes 1572868
  91.6 0.8 copy-start.7
  102.8 0.8 copy-start.3
  137.6 13.2 %copy-start.4 = (f32[256,4,128]{2,0,1:T(8,128)S(1)}, f32[256,4,128]{2,0,1:T(8,128)}, u32[]{:S(2)}) copy-start(f32[256,4,128]{2,0,1:T(8,128)} %copy-done.3) | copy-start | bytes 1572868
  137.6 13.2 %copy-start.6 = (f32[128,4,2,128]{0,3,2,1:T(8,128)S(1)}, f32[128,4,2,128]{0,3,2,1:T(8,128)}, u32[]{:S(2)}) copy-start(f32[128,4,2,128]{0,3,2,1:T(8,128)} %copy-done.5) | copy-start | bytes 1572868
  141.3 8.5 %copy-start.9 = (f32[4,64,4,128]{3,1,0,2:T(8,128)S(1)}, f32[4,64,4,128]{3,1,0,2:T(8,128)}, u32[]{:S(2)}) copy-start(f32[4,64,4,128]{3,1,0,2:T(8,128)} %get-tuple-element.338) | copy-start | bytes 1572868
  155.3 5.2 %collective-permute-start.3 = (bf16[512,32]{0,1:T(8,128)(2,1)S(1)}, bf16[512,32]{0,1:T(8,128)(2,1)S(1)}, u32[]{:S(2)}, u32[]{:S(2)}) collective-permute-start(bf16[512,32]{0,1:T(8,128)(2,1)S(1)} %pad_maximum_fusion.2), channel_id=1, source_target_pairs={{0,16},{8,24},{16,0},{24,8},{1,17},{9,25},{17,1},{25,9},{2,18},{10... | collective-permute-start | bytes 98312 | tf_op jit(solution)/shard_map/ppermute | solution.py:51
  156.9 10.1 %collective-permute-start.1 = (bf16[512,256]{1,0:T(8,128)(2,1)S(1)}, bf16[512,256]{1,0:T(8,128)(2,1)S(1)}, u32[]{:S(2)}, u32[]{:S(2)}) collective-permute-start(bf16[512,256]{1,0:T(8,128)(2,1)S(1)} %pad_maximum_fusion), channel_id=1, source_target_pairs={{0,16},{8,24},{16,0},{24,8},{1,17},{9,25},{17,1},{25,9},{2,18},{10... | collective-permute-start | bytes 786440 | tf_op jit(solution)/shard_map/ppermute | solution.py:51
Sparse Core Ops, SparseCore 0:
  9.8 29.0 all-gather.6
  40.8 35.0 all-gather.4
  177.1 8.2 reduce-scatter.1
where the time goes:
time: 194 us; the launch traced here: 192 us
  blocking collectives  50 us (26%)
  other arithmetic  40.7 us (21%)
  local copies, waits for them, and re-layouts  33.7 us (17%)
  matrix products  30.8 us (16%)
  waiting for transfers between devices  15.6 us (8%)
  between operations  14.3 us (7%)
  starting transfers between devices  6.23 us (3%)
    all_gather x4, blocking collectives, prefix(): lax.all_gather(part.astype(kind), axis)  50 us
    mul x8, other arithmetic, advance(): key_decayed = key_tile * jnp.exp(-inner_block_term)  8.71 us
    reduce_scatter x1, waiting for transfers between devices, local(): lax.psum_scatter((jnp.dot(recurrent_out, w_hg_full, preferred_element_typ...  8.41 us
    dot_general x8, matrix products, advance(): jnp.einsum('mcx,cxn->mcn', damped_query, running_state, precision=largest...  8.11 us
    another operation x8, other arithmetic  7.61 us
    rev x7, local copies, waits for them, and re-layouts, local(): sorted_rows = [jnp.flip(member, axis=0) for member in sorted_rows]  6.92 us
    ppermute x4, waiting for transfers between devices, from_partner(): return lax.ppermute(value, axis, pairs)  6.39 us
    unnamed x35, local copies, waits for them, and re-layouts  6.3 us
  transfers between devices with their start and end apart: 7, of which 3 were waited for; matrix products, arithmetic and copies ran while one was open for 52% of the time, Pallas kernels for 0%

commit v1 on v0

v1 whole, which is shorter than its diff:
```python
import functools

import jax
import jax.numpy as jnp
import numpy as np
from jax import lax
from jax.experimental import pallas as pl
from jax.experimental.pallas import tpu as pltpu
from jax.sharding import PartitionSpec as P

HG_DK = 128
NOPE = 64
ROPE = 32
VDIM = 64
HEAD = NOPE + ROPE
LANES = 128
BLOCK = 128
DECAY_ROWS = 16

norm_eps = 1e-06
rope_base = 10000.0
widest_span = 8

F32 = jnp.float32
BF16 = jnp.bfloat16


def mm(a, b):
    return jnp.dot(a, b, preferred_element_type=F32)


def mm_nt(a, b):
    return lax.dot_general(a, b, (((1,), (1,)), ((), ())), preferred_element_type=F32)


def mm_tn(a, b):
    return lax.dot_general(a, b, (((0,), (0,)), ((), ())), preferred_element_type=F32)


def rope_constants(seq_len, heads):
    half = ROPE // 2
    inverse = (np.float32(rope_base) ** (-np.arange(half, dtype=np.float32) / np.float32(half))).astype(np.float32)
    angles = np.arange(seq_len, dtype=np.float32)[:, None] * inverse[None, :]
    cos_pad = np.zeros((seq_len, LANES), np.float32)
    sin_pad = np.zeros((seq_len, LANES), np.float32)
    cos_pad[:, :NOPE] = 1.0
    cos_pad[:, NOPE:HEAD] = np.tile(np.cos(angles), (1, 2))
    sin_pad[:, NOPE:HEAD] = np.tile(np.sin(angles), (1, 2))
    place = np.zeros((heads * HEAD, heads * LANES), np.float32)
    swap = np.zeros((heads * HEAD, heads * LANES), np.float32)
    for h in range(heads):
        for i in range(HEAD):
            place[h * HEAD + i, h * LANES + i] = 1.0
        for i in range(half):
            a, b = NOPE + i, NOPE + half + i
            swap[h * HEAD + b, h * LANES + a] = -1.0
            swap[h * HEAD + a, h * LANES + b] = 1.0
    return cos_pad, sin_pad, place, swap


def kernel(
    sizes,
    q_ref, f_ref, v_ref, floor_ref, extra_ref, gain_ref, aq_ref, lat_ref, rk_ref,
    lgain_ref, wup_ref, cos_ref, sin_ref, place_ref, swap_ref, w1_ref, w2_ref,
    out_ref, logw_ref,
    lbuf, ssend, srecv, w1buf, w2buf, psend, precv,
    kbuf, vbuf, intra, qf_ref, qb_ref, sf_ref, sb_ref, act,
    l_send, l_recv, s_send, s_recv, w_send, w_recv, x_send, x_recv, own_sem,
):
    n_fs, span = sizes
    tokens, width = q_ref.shape
    heads = width // HG_DK
    att_heads = aq_ref.shape[1] // HEAD
    up = att_heads * (NOPE + VDIM)
    blocks = tokens // BLOCK
    latent_width = lat_ref.shape[1]
    columns = w1_ref.shape[1]
    rows = tokens // 2

    sp, fs, tp = lax.axis_index("sp"), lax.axis_index("fs"), lax.axis_index("tp")
    place = lax.rem(sp, span)
    base = sp - place

    def sp_peer(j):
        return {"sp": base + lax.rem(place + j, span)}

    def fs_peer(j):
        return {"fs": lax.rem(fs + j, n_fs)}

    partner = {"tp": 1 - tp}

    barrier = pltpu.get_barrier_semaphore()
    for j in range(1, n_fs):
        pl.semaphore_signal(barrier, inc=1, device_id=fs_peer(j), device_id_type=pl.DeviceIdType.MESH)
    for j in range(1, span):
        pl.semaphore_signal(barrier, inc=1, device_id=sp_peer(j), device_id_type=pl.DeviceIdType.MESH)
    pl.semaphore_signal(barrier, inc=1, device_id=partner, device_id_type=pl.DeviceIdType.MESH)
    pl.semaphore_wait(barrier, n_fs + span - 1)

    def remote(src, dst, send, recv, device):
        return pltpu.make_async_remote_copy(
            src_ref=src, dst_ref=dst, send_sem=send, recv_sem=recv,
            device_id=device, device_id_type=pl.DeviceIdType.MESH,
        )

    w_copies = []
    for j in range(1, n_fs):
        pair = (
            remote(w1_ref, w1buf.at[j], w_send.at[2 * j], w_recv.at[2 * j], fs_peer(j)),
            remote(w2_ref, w2buf.at[j], w_send.at[2 * j + 1], w_recv.at[2 * j + 1], fs_peer(j)),
        )
        for c in pair:
            c.start()
        w_copies.append(pair)
    own = (
        pltpu.make_async_copy(w1_ref, w1buf.at[0], own_sem.at[0]),
        pltpu.make_async_copy(w2_ref, w2buf.at[0], own_sem.at[1]),
    )
    for c in own:
        c.start()

    offset = pl.multiple_of(place * tokens, tokens)
    cos = cos_ref[pl.ds(offset, tokens), :]
    sin = sin_ref[pl.ds(offset, tokens), :]
    lat = lat_ref[...].astype(F32)
    normed = lat * lax.rsqrt(jnp.mean(lat * lat, axis=-1, keepdims=True) + norm_eps) * lgain_ref[...]
    lbuf[0, :, :latent_width] = normed.astype(BF16)
    rk = rk_ref[...]
    rotated = mm(rk, place_ref[NOPE:HEAD, :LANES]) * cos + mm(rk, swap_ref[NOPE:HEAD, :LANES]) * sin
    lbuf[0, :, latent_width:] = rotated.astype(BF16)
    l_copies = []
    for j in range(1, span):
        c = remote(lbuf.at[0], lbuf.at[j], l_send.at[j], l_recv.at[j], sp_peer(j))
        c.start()
        l_copies.append(c)

    row = lax.broadcasted_iota(jnp.int32, (BLOCK, BLOCK), 0)
    col = lax.broadcasted_iota(jnp.int32, (BLOCK, BLOCK), 1)
    lower = row >= col
    upper = row <= col
    tri = (jnp.where(lower, 1.0, 0.0).astype(BF16), jnp.where(upper, 1.0, 0.0).astype(BF16))
    block_decay = [[[None] * blocks for _ in range(2)] for _ in range(heads)]
    for h in range(heads):
        lanes = slice(h * HG_DK, (h + 1) * HG_DK)
        for b in range(blocks):
            tok = slice(b * BLOCK, (b + 1) * BLOCK)
            q = q_ref[tok, lanes].astype(F32)
            gate = f_ref[tok, lanes].astype(F32)
            v = v_ref[tok, lanes]
            miss = 1.0 / (1.0 + jnp.exp(gate))
            spike = extra_ref[tok, h : h + 1]
            scores = None
            for d in range(2):
                keyed = (1.0 - floor_ref[d : d + 1, lanes]) * miss
                decay = jnp.log1p(-keyed) + spike
                hi = decay.astype(BF16)
                lo = (decay - hi.astype(F32)).astype(BF16)
                run = mm(tri[d], hi) + mm(tri[d], lo)
                mid_at = BLOCK // 2 - 1 if d == 0 else BLOCK // 2
                end_at = BLOCK - 1 if d == 0 else 0
                mid = run[mid_at : mid_at + 1]
                end = run[end_at : end_at + 1]
                grow = jnp.exp(run - mid)
                qd = q * grow
                kd = keyed * jnp.exp(mid - run)
                s = mm_nt(qd.astype(BF16), kd.astype(BF16))
                s = jnp.where(lower if d == 0 else upper, s, 0.0)
                scores = s if scores is None else scores + s
                cross = qf_ref if d == 0 else qb_ref
                cross[tok, lanes] = (qd * jnp.exp(mid)).astype(BF16)
                state = mm_tn(v, (kd * jnp.exp(end - mid)).astype(BF16))
                keep = sf_ref if d == 0 else sb_ref
                keep[b, :, lanes] = state
                block_decay[h][d][b] = jnp.exp(end)
            intra[tok, lanes] = mm(scores.astype(BF16), v)
        for d in range(2):
            keep = sf_ref if d == 0 else sb_ref
            order = range(blocks) if d == 0 else range(blocks - 1, -1, -1)
            total, decay_all = None, None
            for b in order:
                one = keep[b, :, lanes]
                dec = block_decay[h][d][b]
                total = one if total is None else total * dec + one
                decay_all = dec if decay_all is None else decay_all * dec
            ssend[d, :HG_DK, lanes] = total.astype(BF16)
            ssend[d, HG_DK:, lanes] = jnp.broadcast_to(decay_all, (DECAY_ROWS, HG_DK)).astype(BF16)
    s_copies = []
    for j in range(1, span):
        which = jnp.where(place + j < span, 0, 1)
        c = remote(ssend.at[which], srecv.at[j], s_send.at[j], s_recv.at[j], sp_peer(j))
        c.start()
        s_copies.append(c)

    tp_up = pl.multiple_of(tp * up, LANES)
    wup = wup_ref[:, pl.ds(tp_up, up)]
    lane = lax.broadcasted_iota(jnp.int32, (tokens, LANES), 1)
    for j in range(span):
        if j > 0:
            l_copies[j - 1].wait_recv()
        keys = slice(j * tokens, (j + 1) * tokens)
        expanded = mm(lbuf[j, :, :latent_width], wup)
        rot = lbuf[j, :, latent_width:].astype(F32)
        vbuf[keys, :] = expanded.astype(BF16)
        for h in range(att_heads):
            lanes = slice(h * LANES, (h + 1) * LANES)
            kbuf[keys, lanes] = jnp.where(lane < NOPE, expanded[:, lanes], rot).astype(BF16)
    aq = aq_ref[...]
    scale = HEAD ** (-0.5)
    head_lane = lax.broadcasted_iota(jnp.int32, (tokens, att_heads), 1)
    logw = jnp.zeros((tokens, att_heads), F32)
    kept = None
    for h in range(att_heads):
        lanes = slice(h * LANES, (h + 1) * LANES)
        query = mm(aq, place_ref[:, lanes]) * cos + mm(aq, swap_ref[:, lanes]) * sin
        scores = mm_nt(query.astype(BF16), kbuf[:, lanes]) * scale
        peak = jnp.max(scores, axis=-1, keepdims=True)
        weights = jnp.exp(scores - peak)
        totals = jnp.sum(weights, axis=-1, keepdims=True)
        result = mm(weights.astype(BF16), vbuf[:, lanes]) / totals
        logw = jnp.where(head_lane == h, peak + jnp.log(totals), logw)
        if h % 2 == 0:
            kept = pltpu.roll(result, VDIM, 1)
        else:
            at = width + (h // 2) * LANES
            act[:, at : at + LANES] = jnp.where(lane < VDIM, kept, result).astype(BF16)
    logw_ref[...] = logw

    for c in s_copies:
        c.wait_recv()
    for h in range(heads):
        lanes = slice(h * HG_DK, (h + 1) * HG_DK)
        carry_f = jnp.zeros((HG_DK, HG_DK), F32)
        carry_b = jnp.zeros((HG_DK, HG_DK), F32)
        for j in range(span - 1, 0, -1):
            new = carry_f * srecv[j, HG_DK : HG_DK + 1, lanes].astype(F32) + srecv[j, :HG_DK, lanes].astype(F32)
            carry_f = jnp.where(j <= place, new, carry_f)
        for j in range(1, span):
            new = carry_b * srecv[j, HG_DK : HG_DK + 1, lanes].astype(F32) + srecv[j, :HG_DK, lanes].astype(F32)
            carry_b = jnp.where(j > place, new, carry_b)
        starts_f = []
        for b in range(blocks):
            starts_f.append(carry_f)
            carry_f = carry_f * block_decay[h][0][b] + sf_ref[b, :, lanes]
        starts_b = [None] * blocks
        for b in range(blocks - 1, -1, -1):
            starts_b[b] = carry_b
            carry_b = carry_b * block_decay[h][1][b] + sb_ref[b, :, lanes]
        for b in range(blocks):
            tok = slice(b * BLOCK, (b + 1) * BLOCK)
            o = intra[tok, lanes]
            o = o + mm_nt(qf_ref[tok, lanes], starts_f[b].astype(BF16))
            o = o + mm_nt(qb_ref[tok, lanes], starts_b[b].astype(BF16))
            o = o * lax.rsqrt(jnp.mean(o * o, axis=-1, keepdims=True) + norm_eps) * gain_ref[:, lanes]
            act[tok, lanes] = o.astype(BF16)

    mine = pl.multiple_of(tp * rows, rows)
    theirs = pl.multiple_of((1 - tp) * rows, rows)
    kept_rows = []
    x_copies = []

    def finish(j):
        x_copies[j].wait_recv()
        at = pl.multiple_of(lax.rem(fs - j + n_fs, n_fs) * columns, LANES)
        out_ref[:, pl.ds(at, columns)] = (kept_rows[j] + precv[j].astype(F32)).astype(BF16)

    for j in range(n_fs):
        if j == 0:
            for c in own:
                c.wait()
        else:
            for c in w_copies[j - 1]:
                c.wait_recv()
        away = mm(act[pl.ds(theirs, rows), :width], w1buf[j]) + mm(act[pl.ds(theirs, rows), width:], w2buf[j])
        psend[j] = away.astype(BF16)
        c = remote(psend.at[j], precv.at[j], x_send.at[j], x_recv.at[j], partner)
        c.start()
        x_copies.append(c)
        here = mm(act[pl.ds(mine, rows), :width], w1buf[j]) + mm(act[pl.ds(mine, rows), width:], w2buf[j])
        kept_rows.append(here.astype(BF16).astype(F32))
        if j > 0:
            finish(j - 1)
    finish(n_fs - 1)

    for pair in w_copies:
        for c in pair:
            c.wait_send()
    for c in l_copies + s_copies + x_copies:
        c.wait_send()


def local(
    n_fs,
    n_sp,
    recurrent_query,
    forget_logits,
    recurrent_value,
    forget_floor,
    extra_log_decay,
    recurrent_norm_gain,
    attention_query,
    latent,
    rotary_key,
    latent_norm_gain,
    latent_up_weight,
    recurrent_output_weight,
    attention_output_weight,
):
    span = min(n_sp, widest_span)
    tokens, width = recurrent_query.shape[1:]
    heads = width // HG_DK
    att_heads = attention_query.shape[2] // HEAD
    latent_width = latent.shape[2]
    columns = recurrent_output_weight.shape[1]
    att_width = attention_output_weight.shape[0]
    blocks = tokens // BLOCK
    rows = tokens // 2
    cos_pad, sin_pad, place, swap = rope_constants(span * tokens, att_heads)
    vmem = pl.BlockSpec(memory_space=pltpu.VMEM)
    anywhere = pl.BlockSpec(memory_space=pl.ANY)
    dma = pltpu.SemaphoreType.DMA
    mixed, log_weight = pl.pallas_call(
        functools.partial(kernel, (n_fs, span)),
        out_shape=(
            jax.ShapeDtypeStruct((rows, columns * n_fs), BF16),
            jax.ShapeDtypeStruct((tokens, att_heads), F32),
        ),
        in_specs=[vmem] * 15 + [anywhere] * 2,
        out_specs=(vmem, vmem),
        scratch_shapes=[
            pltpu.VMEM((span, tokens, latent_width + LANES), BF16),
            pltpu.VMEM((2, HG_DK + DECAY_ROWS, width), BF16),
            pltpu.VMEM((span, HG_DK + DECAY_ROWS, width), BF16),
            pltpu.VMEM((n_fs, width, columns), BF16),
            pltpu.VMEM((n_fs, att_width, columns), BF16),
            pltpu.VMEM((n_fs, rows, columns), BF16),
            pltpu.VMEM((n_fs, rows, columns), BF16),
            pltpu.VMEM((span * tokens, att_heads * LANES), BF16),
            pltpu.VMEM((span * tokens, att_heads * LANES), BF16),
            pltpu.VMEM((tokens, width), F32),
            pltpu.VMEM((tokens, width), BF16),
            pltpu.VMEM((tokens, width), BF16),
            pltpu.VMEM((blocks, HG_DK, width), F32),
            pltpu.VMEM((blocks, HG_DK, width), F32),
            pltpu.VMEM((tokens, width + att_width), BF16),
            dma((span,)), dma((span,)), dma((span,)), dma((span,)),
            dma((2 * n_fs,)), dma((2 * n_fs,)), dma((n_fs,)), dma((n_fs,)), dma((2,)),
        ],
        compiler_params=pltpu.CompilerParams(
            collective_id=0, has_side_effects=True, vmem_limit_bytes=56 * 2**20
        ),
        name="mixers",
    )(
        recurrent_query[0],
        forget_logits[0],
        recurrent_value[0],
        forget_floor,
        extra_log_decay[0],
        recurrent_norm_gain[None],
        attention_query[0],
        latent[0],
        rotary_key[0],
        latent_norm_gain[None],
        latent_up_weight,
        jnp.asarray(cos_pad),
        jnp.asarray(sin_pad),
        jnp.asarray(place, BF16),
        jnp.asarray(swap, BF16),
        recurrent_output_weight,
        attention_output_weight,
    )
    return mixed[None], log_weight[None]


def solution(mesh):
    placed = (
        P("fs", "sp", "tp"),
        P("fs", "sp", "tp"),
        P("fs", "sp", "tp"),
        P(None, "tp"),
        P("fs", "sp", "tp"),
        P("tp"),
        P("fs", "sp", "tp"),
        P("fs", "sp", None),
        P("fs", "sp", None),
        P(),
        P(),
        P("tp", "fs"),
        P("tp", "fs"),
    )
    return jax.shard_map(
        functools.partial(local, mesh.shape["fs"], mesh.shape["sp"]),
        mesh=mesh,
        in_specs=placed,
        out_specs=(P("fs", ("sp", "tp"), None), P("fs", "sp", "tp")),
        check_vma=False,
    )
```

time: 194 us -> 52.7 us (0.27)
  blocking collectives: 50 us -> 0 us
  Pallas kernels: 0 us -> 46.1 us
  other arithmetic: 40.7 us -> 0 us
  matrix products: 30.8 us -> 0 us
  local copies, waits for them, and re-layouts: 33.7 us -> 5.71 us
  waiting for transfers between devices: 15.6 us -> 0 us
  between operations: 14.3 us -> 0.65 us
  starting transfers between devices: 6.23 us -> 0 us
    all_gather x4 -> x0, blocking collectives: 50 us -> none  [prefix(): lax.all_gather(part.astype(kind), axis)]
    pallas_call x0 -> x1, Pallas kernels: none -> 46.1 us  [local(): pl.pallas_call(functools.partial(kernel, (n_fs, span)), out_shape=(jax.Sh...]
    dot_general x39 -> x0, matrix products: 30.8 us -> none  [the longest x8 8.11 us: advance(): jnp.einsum('mcx,cxn->mcn', damped_query, running_state, precision=largest...]
    another operation x16 -> x0, other arithmetic: 11.9 us -> none
    rev x8 -> x0, local copies, waits for them, and re-layouts: 10.7 us -> none  [the longest x7 6.92 us: local(): sorted_rows = [jnp.flip(member, axis=0) for member in sorted_rows]]
    mul x9 -> x0, other arithmetic: 9.52 us -> none  [the longest x8 8.71 us: advance(): key_decayed = key_tile * jnp.exp(-inner_block_term)]
    reduce_scatter x1 -> x0, waiting for transfers between devices: 8.41 us -> none  [local(): lax.psum_scatter((jnp.dot(recurrent_out, w_hg_full, preferred_element_typ...]
    convert_element_type x18 -> x0, other arithmetic: 7.08 us -> none  [the longest x8 2.78 us: hop(): part[at].astype(own.dtype)]
  transfers between devices with their start and end apart: 7 -> 0, of which waited for: 3 -> 0; matrix products, arithmetic and copies ran while one was open for 52% -> 0% of each run, Pallas kernels for 0% -> 0%
where the time goes in v1:
time: 52.7 us; the launch traced here: 52.4 us
  Pallas kernels  46.1 us (87%)
  local copies, waits for them, and re-layouts  5.71 us (11%)
  between operations  0.65 us (1%)
    pallas_call x1, Pallas kernels, local(): pl.pallas_call(functools.partial(kernel, (n_fs, span)), out_shape=(jax.Sh...  46.1 us
    unnamed x6, local copies, waits for them, and re-layouts  5.71 us

profile of v1, /device:TPU:0, one launch (start us, length us, event | category | flops | bytes accessed | tf_op | source)
XLA Modules:
  0.0 52.4 jit_solution(15140292350943330795)
XLA Ops:
  0.6 0.0 copy-start
  0.6 1.5 %copy.20 = bf16[1,256,32]{2,1,0:T(8,128)(2,1)} copy(bf16[1,256,32]{1,2,0:T(8,128)(2,1)} %param.25) | data formatting | bytes 32768 | tf_op args[8]
  2.1 0.0 copy-done
  2.1 0.8 %copy.19 = f32[1,256,4]{2,1,0:T(8,128)} copy(f32[1,256,4]{1,2,0:T(4,128)S(1)} %copy-done) | data formatting | bytes 8192 | tf_op args[4]
  2.9 46.1 %mixers.1 = (bf16[128,2048]{1,0:T(8,128)(2,1)}, f32[256,4]{1,0:T(8,128)}) custom-call(bf16[256,512]{1,0:T(8,128)(2,1)} %bitcast.14, bf16[256,512]{1,0:T(8,128)(2,1)} %bitcast.15, bf16[256,512]{1,0:T(8,128)(2,1)} %bitcast.16, f32[2,512]{1,0:T(2,128)} %floor_ref.1, f32[256,4]{1,0:T(8,128)} %bitcast.12, f32[1,512]{1,0:T(1,128)} %bitcast.20, ...), custom_call_target="tpu_custom_call" | custom-call | tf_op jit(solution)/shard_map/mixers/pallas_call | solution.py:321
  49.0 1.6 %copy.21 = f32[1,256,4]{1,2,0:T(4,128)} copy(f32[1,256,4]{2,1,0:T(8,128)} %bitcast.18) | data formatting | bytes 8192
  50.5 1.9 %copy.23 = bf16[1,128,2048]{2,1,0:T(8,128)(2,1)} copy(bf16[1,128,2048]{2,1,0:T(8,128)(2,1)} %bitcast.11) | data formatting | bytes 1048576
Async XLA Ops:
  0.6 1.5 %copy-start = (f32[1,256,4]{1,2,0:T(4,128)S(1)}, f32[1,256,4]{1,2,0:T(4,128)}, u32[]{:S(2)}) copy-start(f32[1,256,4]{1,2,0:T(4,128)} %param.21) | copy-start | bytes 12292

commit v2 on v1

--- a/solution.py
+++ b/solution.py
@@ -15,7 +15,6 @@
 HEAD = NOPE + ROPE
 LANES = 128
 BLOCK = 128
-DECAY_ROWS = 16
 
 norm_eps = 1e-06
 rope_base = 10000.0
@@ -35,6 +34,15 @@
 
 def mm_tn(a, b):
     return lax.dot_general(a, b, (((0,), (0,)), ((), ())), preferred_element_type=F32)
+
+
+def flip_bits(value, mask):
+    bit = 1
+    while bit <= mask:
+        if mask & bit:
+            value = value + bit - 2 * bit * lax.rem(value // bit, 2)
+        bit *= 2
+    return value
 
 
 def rope_constants(seq_len, heads):
@@ -64,8 +72,9 @@
     lgain_ref, wup_ref, cos_ref, sin_ref, place_ref, swap_ref, w1_ref, w2_ref,
     out_ref, logw_ref,
     lbuf, ssend, srecv, w1buf, w2buf, psend, precv,
-    kbuf, vbuf, intra, qf_ref, qb_ref, sf_ref, sb_ref, act,
-    l_send, l_recv, s_send, s_recv, w_send, w_recv, x_send, x_recv, own_sem,
+    kbuf, vbuf, intra, qf_ref, qb_ref, sf_ref, sb_ref, act, whole_state, whole_decay,
+    l_send, l_recv, f_send, f_recv, s_send, s_recv, w_send, w_recv, r_send, r_recv,
+    x_send, x_recv, own_sem,
 ):
     n_fs, span = sizes
     tokens, width = q_ref.shape
@@ -85,7 +94,7 @@
         return {"sp": base + lax.rem(place + j, span)}
 
     def fs_peer(j):
-        return {"fs": lax.rem(fs + j, n_fs)}
+        return {"fs": flip_bits(fs, j)}
 
     partner = {"tp": 1 - tp}
 
@@ -103,15 +112,32 @@
             device_id=device, device_id_type=pl.DeviceIdType.MESH,
         )
 
-    w_copies = []
-    for j in range(1, n_fs):
-        pair = (
-            remote(w1_ref, w1buf.at[j], w_send.at[2 * j], w_recv.at[2 * j], fs_peer(j)),
-            remote(w2_ref, w2buf.at[j], w_send.at[2 * j + 1], w_recv.at[2 * j + 1], fs_peer(j)),
-        )
-        for c in pair:
+    parity = lax.rem(place, 2)
+    pair = {"sp": base + flip_bits(place, 1)}
+    far = [j for j in range(1, n_fs) if j & (j - 1) and span % 2 == 0]
+    near = [j for j in range(1, n_fs) if j not in far]
+    weights = ((w1_ref, w1buf), (w2_ref, w2buf))
+
+    def half_rows(ref):
+        size = ref.shape[-2] // 2
+        return pl.ds(pl.multiple_of(parity * size, size), size)
+
+    w_copies = {}
+    for j in far + near:
+        pieces = []
+        for k, (src, dst) in enumerate(weights):
+            there = dst.at[j]
+            if j in far:
+                src, there = src.at[half_rows(src)], there.at[half_rows(dst)]
+            c = remote(src, there, w_send.at[2 * j + k], w_recv.at[2 * j + k], fs_peer(j))
             c.start()
-        w_copies.append(pair)
+            pieces.append(c)
+        w_copies[j] = pieces
+    relays = {j: [
+        remote(dst.at[j, half_rows(dst)], dst.at[j, half_rows(dst)],
+               r_send.at[2 * j + k], r_recv.at[2 * j + k], pair)
+        for k, (_, dst) in enumerate(weights)
+    ] for j in far}
     own = (
         pltpu.make_async_copy(w1_ref, w1buf.at[0], own_sem.at[0]),
         pltpu.make_async_copy(w2_ref, w2buf.at[0], own_sem.at[1]),
@@ -126,11 +152,12 @@
     normed = lat * lax.rsqrt(jnp.mean(lat * lat, axis=-1, keepdims=True) + norm_eps) * lgain_ref[...]
     lbuf[0, :, :latent_width] = normed.astype(BF16)
     rk = rk_ref[...]
-    rotated = mm(rk, place_ref[NOPE:HEAD, :LANES]) * cos + mm(rk, swap_ref[NOPE:HEAD, :LANES]) * sin
+    rotated = mm_tn(rk, place_ref[NOPE:HEAD, :LANES]) * cos + mm_tn(rk, swap_ref[NOPE:HEAD, :LANES]) * sin
     lbuf[0, :, latent_width:] = rotated.astype(BF16)
+    my_rows = pl.ds(pl.multiple_of(tp * rows, rows), rows)
     l_copies = []
     for j in range(1, span):
-        c = remote(lbuf.at[0], lbuf.at[j], l_send.at[j], l_recv.at[j], sp_peer(j))
+        c = remote(lbuf.at[0, my_rows], lbuf.at[j, my_rows], l_send.at[j], l_recv.at[j], sp_peer(j))
         c.start()
         l_copies.append(c)
 
@@ -139,6 +166,12 @@
     lower = row >= col
     upper = row <= col
     tri = (jnp.where(lower, 1.0, 0.0).astype(BF16), jnp.where(upper, 1.0, 0.0).astype(BF16))
+    spikes = lax.dot_general(
+        extra_ref[...],
+        jnp.where(
+            lax.broadcasted_iota(jnp.int32, (heads, width), 0)
+            == lax.broadcasted_iota(jnp.int32, (heads, width), 1) // HG_DK, 1.0, 0.0),
+        (((0,), (0,)), ((), ())), precision=lax.Precision.HIGHEST, preferred_element_type=F32)
     block_decay = [[[None] * blocks for _ in range(2)] for _ in range(heads)]
     for h in range(heads):
         lanes = slice(h * HG_DK, (h + 1) * HG_DK)
@@ -148,7 +181,7 @@
             gate = f_ref[tok, lanes].astype(F32)
             v = v_ref[tok, lanes]
             miss = 1.0 / (1.0 + jnp.exp(gate))
-            spike = extra_ref[tok, h : h + 1]
+            spike = spikes[tok, lanes]
             scores = None
             for d in range(2):
                 keyed = (1.0 - floor_ref[d : d + 1, lanes]) * miss
@@ -182,21 +215,62 @@
                 dec = block_decay[h][d][b]
                 total = one if total is None else total * dec + one
                 decay_all = dec if decay_all is None else decay_all * dec
-            ssend[d, :HG_DK, lanes] = total.astype(BF16)
-            ssend[d, HG_DK:, lanes] = jnp.broadcast_to(decay_all, (DECAY_ROWS, HG_DK)).astype(BF16)
-    s_copies = []
+            whole_state[d, h] = total
+            whole_decay[d, h] = jnp.broadcast_to(decay_all, (8, HG_DK))
+
+    first = jnp.where(2 * place < span, 0, 1)
+
+    def link(d, h):
+        towards = jnp.clip(place + 1 - 2 * d, 0, span - 1)
+        return remote(ssend.at[d, h], srecv.at[d, h], s_send.at[d, h], s_recv.at[d, h],
+                      {"sp": base + towards})
+
+    def has_previous(d):
+        return jnp.where(d == 0, place, span - 1 - place) > 0
+
+    def has_next(d):
+        return jnp.where(d == 0, span - 1 - place, place) > 0
+
+    def pass_on(d):
+        for h in range(heads):
+            @pl.when(has_previous(d))
+            def _():
+                link(d, h).wait_recv()
+
+            @pl.when(jnp.logical_not(has_previous(d)))
+            def _():
+                srecv[d, h] = jnp.zeros((HG_DK, HG_DK), BF16)
+
+            @pl.when(has_next(d))
+            def _():
+                reached = srecv[d, h].astype(F32) * whole_decay[d, h, 0:1] + whole_state[d, h]
+                ssend[d, h] = reached.astype(BF16)
+                link(d, h).start()
+
+    pass_on(first)
+
+    forwards = []
     for j in range(1, span):
-        which = jnp.where(place + j < span, 0, 1)
-        c = remote(ssend.at[which], srecv.at[j], s_send.at[j], s_recv.at[j], sp_peer(j))
+        l_copies[j - 1].wait_recv()
+        c = remote(lbuf.at[j, my_rows], lbuf.at[j, my_rows], f_send.at[j], f_recv.at[j], partner)
         c.start()
-        s_copies.append(c)
+        forwards.append(c)
+
+    @pl.when(has_next(1 - first))
+    def _():
+        pass_on(1 - first)
+
+    for j in far:
+        for c, r in zip(w_copies[j], relays[j]):
+            c.wait_recv()
+            r.start()
 
     tp_up = pl.multiple_of(tp * up, LANES)
     wup = wup_ref[:, pl.ds(tp_up, up)]
     lane = lax.broadcasted_iota(jnp.int32, (tokens, LANES), 1)
     for j in range(span):
         if j > 0:
-            l_copies[j - 1].wait_recv()
+            forwards[j - 1].wait_recv()
         keys = slice(j * tokens, (j + 1) * tokens)
         expanded = mm(lbuf[j, :, :latent_width], wup)
         rot = lbuf[j, :, latent_width:].astype(F32)
@@ -206,8 +280,7 @@
             kbuf[keys, lanes] = jnp.where(lane < NOPE, expanded[:, lanes], rot).astype(BF16)
     aq = aq_ref[...]
     scale = HEAD ** (-0.5)
-    head_lane = lax.broadcasted_iota(jnp.int32, (tokens, att_heads), 1)
-    logw = jnp.zeros((tokens, att_heads), F32)
+    logw = jnp.zeros((tokens, LANES), F32)
     kept = None
     for h in range(att_heads):
         lanes = slice(h * LANES, (h + 1) * LANES)
@@ -217,26 +290,22 @@
         weights = jnp.exp(scores - peak)
         totals = jnp.sum(weights, axis=-1, keepdims=True)
         result = mm(weights.astype(BF16), vbuf[:, lanes]) / totals
-        logw = jnp.where(head_lane == h, peak + jnp.log(totals), logw)
+        logw = jnp.where(lane == h, peak + jnp.log(totals), logw)
         if h % 2 == 0:
             kept = pltpu.roll(result, VDIM, 1)
         else:
             at = width + (h // 2) * LANES
             act[:, at : at + LANES] = jnp.where(lane < VDIM, kept, result).astype(BF16)
-    logw_ref[...] = logw
-
-    for c in s_copies:
-        c.wait_recv()
+    logw_ref[...] = jnp.transpose(logw)[:att_heads]
+
+    @pl.when(jnp.logical_not(has_next(1 - first)))
+    def _():
+        pass_on(1 - first)
+
     for h in range(heads):
         lanes = slice(h * HG_DK, (h + 1) * HG_DK)
-        carry_f = jnp.zeros((HG_DK, HG_DK), F32)
-        carry_b = jnp.zeros((HG_DK, HG_DK), F32)
-        for j in range(span - 1, 0, -1):
-            new = carry_f * srecv[j, HG_DK : HG_DK + 1, lanes].astype(F32) + srecv[j, :HG_DK, lanes].astype(F32)
-            carry_f = jnp.where(j <= place, new, carry_f)
-        for j in range(1, span):
-            new = carry_b * srecv[j, HG_DK : HG_DK + 1, lanes].astype(F32) + srecv[j, :HG_DK, lanes].astype(F32)
-            carry_b = jnp.where(j > place, new, carry_b)
+        carry_f = srecv[0, h].astype(F32)
+        carry_b = srecv[1, h].astype(F32)
         starts_f = []
         for b in range(blocks):
             starts_f.append(carry_f)
@@ -260,7 +329,7 @@
 
     def finish(j):
         x_copies[j].wait_recv()
-        at = pl.multiple_of(lax.rem(fs - j + n_fs, n_fs) * columns, LANES)
+        at = pl.multiple_of(flip_bits(fs, j) * columns, LANES)
         out_ref[:, pl.ds(at, columns)] = (kept_rows[j] + precv[j].astype(F32)).astype(BF16)
 
     for j in range(n_fs):
@@ -268,7 +337,7 @@
             for c in own:
                 c.wait()
         else:
-            for c in w_copies[j - 1]:
+            for c in relays[j] if j in far else w_copies[j]:
                 c.wait_recv()
         away = mm(act[pl.ds(theirs, rows), :width], w1buf[j]) + mm(act[pl.ds(theirs, rows), width:], w2buf[j])
         psend[j] = away.astype(BF16)
@@ -281,11 +350,16 @@
             finish(j - 1)
     finish(n_fs - 1)
 
-    for pair in w_copies:
-        for c in pair:
+    for pieces in list(w_copies.values()) + list(relays.values()):
+        for c in pieces:
             c.wait_send()
-    for c in l_copies + s_copies + x_copies:
+    for c in l_copies + forwards + x_copies:
         c.wait_send()
+    for d in range(2):
+        for h in range(heads):
+            @pl.when(has_next(d))
+            def _():
+                link(d, h).wait_send()
 
 
 def local(
@@ -322,14 +396,14 @@
         functools.partial(kernel, (n_fs, span)),
         out_shape=(
             jax.ShapeDtypeStruct((rows, columns * n_fs), BF16),
-            jax.ShapeDtypeStruct((tokens, att_heads), F32),
+            jax.ShapeDtypeStruct((att_heads, tokens), F32),
         ),
         in_specs=[vmem] * 15 + [anywhere] * 2,
         out_specs=(vmem, vmem),
         scratch_shapes=[
             pltpu.VMEM((span, tokens, latent_width + LANES), BF16),
-            pltpu.VMEM((2, HG_DK + DECAY_ROWS, width), BF16),
-            pltpu.VMEM((span, HG_DK + DECAY_ROWS, width), BF16),
+            pltpu.VMEM((2, heads, HG_DK, HG_DK), BF16),
+            pltpu.VMEM((2, heads, HG_DK, HG_DK), BF16),
             pltpu.VMEM((n_fs, width, columns), BF16),
             pltpu.VMEM((n_fs, att_width, columns), BF16),
             pltpu.VMEM((n_fs, rows, columns), BF16),
@@ -342,8 +416,11 @@
             pltpu.VMEM((blocks, HG_DK, width), F32),
             pltpu.VMEM((blocks, HG_DK, width), F32),
             pltpu.VMEM((tokens, width + att_width), BF16),
-            dma((span,)), dma((span,)), dma((span,)), dma((span,)),
-            dma((2 * n_fs,)), dma((2 * n_fs,)), dma((n_fs,)), dma((n_fs,)), dma((2,)),
+            pltpu.VMEM((2, heads, HG_DK, HG_DK), F32),
+            pltpu.VMEM((2, heads, 8, HG_DK), F32),
+            dma((span,)), dma((span,)), dma((span,)), dma((span,)), dma((2, heads)), dma((2, heads)),
+            dma((2 * n_fs,)), dma((2 * n_fs,)), dma((2 * n_fs,)), dma((2 * n_fs,)),
+            dma((n_fs,)), dma((n_fs,)), dma((2,)),
         ],
         compiler_params=pltpu.CompilerParams(
             collective_id=0, has_side_effects=True, vmem_limit_bytes=56 * 2**20
@@ -354,11 +431,11 @@
         forget_logits[0],
         recurrent_value[0],
         forget_floor,
-        extra_log_decay[0],
+        extra_log_decay[0].T,
         recurrent_norm_gain[None],
         attention_query[0],
         latent[0],
-        rotary_key[0],
+        rotary_key[0].T,
         latent_norm_gain[None],
         latent_up_weight,
         jnp.asarray(cos_pad),
@@ -368,7 +445,7 @@
         recurrent_output_weight,
         attention_output_weight,
     )
-    return mixed[None], log_weight[None]
+    return mixed[None], log_weight.T[None]
 
 
 def solution(mesh):

time: 52.7 us -> 42.1 us (0.80)
  Pallas kernels: 46.1 us -> 38.8 us
  local copies, waits for them, and re-layouts: 5.71 us -> 2.48 us
    pallas_call x1, Pallas kernels: 46.1 us -> 38.8 us  [local(): pl.pallas_call(functools.partial(kernel, (n_fs, span)), out_shape=(jax.Sh...]
    unnamed x6 -> x4, local copies, waits for them, and re-layouts: 5.71 us -> 2.48 us
where the time goes in v2:
time: 42.1 us; the launch traced here: 41.9 us
  Pallas kernels  38.8 us (92%)
  local copies, waits for them, and re-layouts  2.48 us (6%)
  between operations  0.65 us (2%)
    pallas_call x1, Pallas kernels, local(): pl.pallas_call(functools.partial(kernel, (n_fs, span)), out_shape=(jax.Sh...  38.8 us
    unnamed x4, local copies, waits for them, and re-layouts  2.48 us

profile of v2, /device:TPU:0, one launch (start us, length us, event | category | flops | bytes accessed | tf_op | source)
XLA Modules:
  0.0 41.9 jit_solution(2199201381174137100)
XLA Ops:
  0.6 38.8 %mixers.1 = (bf16[128,2048]{1,0:T(8,128)(2,1)}, f32[4,256]{1,0:T(4,128)}) custom-call(bf16[256,512]{1,0:T(8,128)(2,1)} %bitcast.18, bf16[256,512]{1,0:T(8,128)(2,1)} %bitcast.19, bf16[256,512]{1,0:T(8,128)(2,1)} %bitcast.20, f32[2,512]{1,0:T(2,128)} %floor_ref.1, f32[4,256]{1,0:T(4,128)} %bitcast.25, f32[1,512]{1,0:T(1,128)} %bitcast.26, ...), custom_call_target="tpu_custom_call" | custom-call | tf_op jit(solution)/shard_map/mixers/pallas_call | solution.py:395
  39.5 0.0 copy-start
  39.5 1.9 %copy.21 = bf16[1,128,2048]{2,1,0:T(8,128)(2,1)} copy(bf16[1,128,2048]{2,1,0:T(8,128)(2,1)} %bitcast.17) | data formatting | bytes 1048576
  41.3 0.0 copy-done
  41.3 0.6 %copy.22 = f32[1,256,4]{1,2,0:T(4,128)} copy(f32[1,256,4]{1,2,0:T(4,128)S(1)} %bitcast.24) | data formatting | bytes 8192
Async XLA Ops:
  39.5 1.9 %copy-start = (f32[4,256]{1,0:T(4,128)S(1)}, f32[4,256]{1,0:T(4,128)}, u32[]{:S(2)}) copy-start(f32[4,256]{1,0:T(4,128)} %get-tuple-element.5) | copy-start | bytes 12292

commit v3 on v2

--- a/solution.py
+++ b/solution.py
@@ -19,6 +19,7 @@
 norm_eps = 1e-06
 rope_base = 10000.0
 widest_span = 8
+LOG2_E = 1.4426950408889634
 
 F32 = jnp.float32
 BF16 = jnp.bfloat16
@@ -247,6 +248,11 @@
                 ssend[d, h] = reached.astype(BF16)
                 link(d, h).start()
 
+    for j in far:
+        for c, r in zip(w_copies[j], relays[j]):
+            c.wait_recv()
+            r.start()
+
     pass_on(first)
 
     forwards = []
@@ -259,11 +265,6 @@
     @pl.when(has_next(1 - first))
     def _():
         pass_on(1 - first)
-
-    for j in far:
-        for c, r in zip(w_copies[j], relays[j]):
-            c.wait_recv()
-            r.start()
 
     tp_up = pl.multiple_of(tp * up, LANES)
     wup = wup_ref[:, pl.ds(tp_up, up)]
@@ -285,9 +286,10 @@
     for h in range(att_heads):
         lanes = slice(h * LANES, (h + 1) * LANES)
         query = mm(aq, place_ref[:, lanes]) * cos + mm(aq, swap_ref[:, lanes]) * sin
-        scores = mm_nt(query.astype(BF16), kbuf[:, lanes]) * scale
-        peak = jnp.max(scores, axis=-1, keepdims=True)
-        weights = jnp.exp(scores - peak)
+        scores = mm_nt(query.astype(BF16), kbuf[:, lanes])
+        top = jnp.max(scores, axis=-1, keepdims=True)
+        peak = top * scale
+        weights = jnp.exp2((scores - top) * (scale * LOG2_E))
         totals = jnp.sum(weights, axis=-1, keepdims=True)
         result = mm(weights.astype(BF16), vbuf[:, lanes]) / totals
         logw = jnp.where(lane == h, peak + jnp.log(totals), logw)
@@ -324,36 +326,53 @@
 
     mine = pl.multiple_of(tp * rows, rows)
     theirs = pl.multiple_of((1 - tp) * rows, rows)
-    kept_rows = []
-    x_copies = []
+    kept_rows = {}
+    x_copies = {}
+
+    def part(at, j, k):
+        rows_at = pl.ds(at, rows)
+        if k == 0:
+            return mm(act[rows_at, :width], w1buf[j])
+        return mm(act[rows_at, width:], w2buf[j])
+
+    def arrive(j, k):
+        if j == 0:
+            own[k].wait()
+        else:
+            (relays[j] if j in far else w_copies[j])[k].wait_recv()
+
+    def exchange(j, away, here):
+        psend[j] = away.astype(BF16)
+        c = remote(psend.at[j], precv.at[j], x_send.at[j], x_recv.at[j], partner)
+        c.start()
+        x_copies[j] = c
+        kept_rows[j] = (here if here is not None else part(mine, j, 0) + part(mine, j, 1)).astype(BF16).astype(F32)
 
     def finish(j):
         x_copies[j].wait_recv()
         at = pl.multiple_of(flip_bits(fs, j) * columns, LANES)
         out_ref[:, pl.ds(at, columns)] = (kept_rows[j] + precv[j].astype(F32)).astype(BF16)
 
-    for j in range(n_fs):
-        if j == 0:
-            for c in own:
-                c.wait()
-        else:
-            for c in relays[j] if j in far else w_copies[j]:
-                c.wait_recv()
-        away = mm(act[pl.ds(theirs, rows), :width], w1buf[j]) + mm(act[pl.ds(theirs, rows), width:], w2buf[j])
-        psend[j] = away.astype(BF16)
-        c = remote(psend.at[j], precv.at[j], x_send.at[j], x_recv.at[j], partner)
-        c.start()
-        x_copies.append(c)
-        here = mm(act[pl.ds(mine, rows), :width], w1buf[j]) + mm(act[pl.ds(mine, rows), width:], w2buf[j])
-        kept_rows.append(here.astype(BF16).astype(F32))
-        if j > 0:
-            finish(j - 1)
-    finish(n_fs - 1)
+    for j in [0] + far:
+        arrive(j, 0)
+        arrive(j, 1)
+        exchange(j, part(theirs, j, 0) + part(theirs, j, 1), None)
+    begun = {}
+    for j in near:
+        arrive(j, 0)
+        begun[j] = (part(theirs, j, 0), part(mine, j, 0))
+    for j in [0] + far:
+        finish(j)
+    for j in near:
+        arrive(j, 1)
+        exchange(j, begun[j][0] + part(theirs, j, 1), begun[j][1] + part(mine, j, 1))
+    for j in near:
+        finish(j)
 
     for pieces in list(w_copies.values()) + list(relays.values()):
         for c in pieces:
             c.wait_send()
-    for c in l_copies + forwards + x_copies:
+    for c in l_copies + forwards + list(x_copies.values()):
         c.wait_send()
     for d in range(2):
         for h in range(heads):

time: 42.1 us -> 42.3 us (level)
  no operation moved by 1% of the time
where the time goes in v3:
time: 42.3 us; the launch traced here: 42.1 us
  Pallas kernels  39 us (92%)
  local copies, waits for them, and re-layouts  2.48 us (6%)
  between operations  0.65 us (2%)
    pallas_call x1, Pallas kernels, local(): pl.pallas_call(functools.partial(kernel, (n_fs, span)), out_shape=(jax.Sh...  39 us
    unnamed x4, local copies, waits for them, and re-layouts  2.48 us

profile of v3, /device:TPU:0, one launch (start us, length us, event | category | flops | bytes accessed | tf_op | source)
XLA Modules:
  0.0 42.1 jit_solution(16380037118693980419)
XLA Ops:
  0.6 39.0 %mixers.1 = (bf16[128,2048]{1,0:T(8,128)(2,1)}, f32[4,256]{1,0:T(4,128)}) custom-call(bf16[256,512]{1,0:T(8,128)(2,1)} %bitcast.18, bf16[256,512]{1,0:T(8,128)(2,1)} %bitcast.19, bf16[256,512]{1,0:T(8,128)(2,1)} %bitcast.20, f32[2,512]{1,0:T(2,128)} %floor_ref.1, f32[4,256]{1,0:T(4,128)} %bitcast.25, f32[1,512]{1,0:T(1,128)} %bitcast.26, ...), custom_call_target="tpu_custom_call" | custom-call | tf_op jit(solution)/shard_map/mixers/pallas_call | solution.py:414
  39.6 0.0 copy-start
  39.7 1.9 %copy.21 = bf16[1,128,2048]{2,1,0:T(8,128)(2,1)} copy(bf16[1,128,2048]{2,1,0:T(8,128)(2,1)} %bitcast.17) | data formatting | bytes 1048576
  41.5 0.0 copy-done
  41.5 0.6 %copy.22 = f32[1,256,4]{1,2,0:T(4,128)} copy(f32[1,256,4]{1,2,0:T(4,128)S(1)} %bitcast.24) | data formatting | bytes 8192
Async XLA Ops:
  39.6 1.9 %copy-start = (f32[4,256]{1,0:T(4,128)S(1)}, f32[4,256]{1,0:T(4,128)}, u32[]{:S(2)}) copy-start(f32[4,256]{1,0:T(4,128)} %get-tuple-element.5) | copy-start | bytes 12292
